TPU v7x, 128 devices: a whole 4x4x4 slice. The times are simulated.
128 devices in a mesh: rep: 2 (over z_hi), fs: 32 (over z_lo, y, x), tp: 2 (over core).
Axes of the slice: x: 4, y: 4, z: 4 (z_hi: 2, z_lo: 2; z = z_hi * 2 + z_lo), core: 2. Of those that a mesh axis runs over, the one named last changes fastest.
Arguments:
- tokens: bfloat16 [256, 64, 2048], P('tp', ('rep', 'fs')), may hold values from -6 to 6
- mix_gain: float32 [2048], replicated, may hold values from 0.1 to 1.9
- value_weight: bfloat16 [2048, 1024], P('fs', 'tp'), may hold values from -0.125 to 0.125
- gate_weight: bfloat16 [2048, 1024], P('fs', 'tp'), may hold values from -0.125 to 0.125
- conv_taps: float32 [31, 1024], P(None, 'tp'), may hold values from -1 to 1
- head_gain: float32 [1024], P('tp'), may hold values from 0.1 to 1.9
- out_weight: bfloat16 [1024, 2048], P('tp', 'fs'), may hold values from -0.1875 to 0.1875
- ffn_gain: float32 [2048], replicated, may hold values from 0.1 to 1.9
- ffn_gate_weight: bfloat16 [2048, 3072], P('fs', 'tp'), may hold values from -0.125 to 0.125
- ffn_up_weight: bfloat16 [2048, 3072], P('fs', 'tp'), may hold values from -0.125 to 0.125
- down_weight: bfloat16 [3072, 2048], P('tp', 'fs'), may hold values from -0.109375 to 0.109375
Outputs:
- layer_out: bfloat16 [256, 64, 2048], P('tp', ('rep', 'fs'))
All inputs are finite; a program needn't handle non-finite values.
Results may differ from a plain program's by a relative error of at most 0.012.
Values may be sent and summed in bfloat16 or wider, within the bound.
No kernel may reach another device: no remote copies, remote signals or barrier semaphores. Data moves between devices by JAX's collectives and lax.ppermute only.
A program may use at most 128 MiB of HBM per device.

v0:
```python
import jax
import jax.numpy as jnp
from jax import lax
from jax.sharding import PartitionSpec as P

HEAD_DIM = 128
norm_eps = 1e-06
group_eps = 1e-05


def from_everyone(value, axis):
    count = lax.axis_size(axis)
    return lax.all_to_all(
        jnp.broadcast_to(value[None], (count, *value.shape)), axis, 0, 0, tiled=True
    )


def laid_out(parts, dim):
    lengths = list(parts.shape[1:])
    lengths[dim] *= parts.shape[0]
    return jnp.moveaxis(parts, 0, dim).reshape(lengths)


def gather_directly(value, axis, dim):
    parts = from_everyone(value, axis)
    return laid_out(parts, dim)


def sent_together(arrays, axis, dim, along):
    both = jnp.concatenate(arrays, axis=along)
    out, at, finished = (lax.all_gather(both, axis, axis=dim, tiled=True), 0, [])
    for a in arrays:
        finished.append(lax.slice_in_dim(out, at, at + a.shape[along], axis=along))
        at += a.shape[along]
    return tuple(finished)


def cut_along(value, dim, count):
    before, after = (value.shape[:dim], value.shape[dim + 1 :])
    return jnp.moveaxis(value.reshape(*before, count, -1, *after), dim, 0)


def sent_and_summed(value, axis, dim):
    parts = cut_along(value, dim, lax.axis_size(axis))
    arrived = lax.all_to_all(parts, axis, split_axis=0, concat_axis=0, tiled=True)
    return arrived.astype(jnp.float32).sum(axis=0)


def rms_scale(matrix, scales):
    return matrix * lax.rsqrt(jnp.mean(matrix * matrix, axis=-1, keepdims=True) + norm_eps) * scales


def body(
    tokens,
    mix_gain,
    value_weight,
    gate_weight,
    conv_taps,
    head_gain,
    out_weight,
    ffn_gain,
    ffn_gate_weight,
    ffn_up_weight,
    down_weight,
):
    local_len, seq_count, model_width = tokens.shape
    own_rows = local_len * seq_count
    whole_rows = gather_directly(tokens, "tp", 0)
    full_len = whole_rows.shape[0]
    normed = rms_scale(whole_rows.reshape(-1, model_width).astype(jnp.float32), mix_gain).astype(
        jnp.bfloat16
    )
    channels = value_weight.shape[1]
    pieces = sent_together((value_weight, gate_weight), "fs", 0, 1)
    sliced = normed
    value_rows = jnp.dot(sliced, pieces[0], preferred_element_type=jnp.float32)
    gate_rows = jnp.dot(sliced, pieces[1], preferred_element_type=jnp.float32)
    glu_rows = (
        (value_rows * jax.nn.sigmoid(gate_rows))
        .astype(jnp.bfloat16)
        .reshape(full_len, seq_count, channels)
    )
    kernel = conv_taps.shape[0]
    conved = lax.conv_general_dilated(
        glu_rows.astype(jnp.float32),
        conv_taps[:, None, :],
        (1,),
        [(kernel // 2, kernel // 2)],
        dimension_numbers=("WNC", "WIO", "WNC"),
        feature_group_count=channels,
        precision=lax.Precision.HIGHEST,
    )
    grouped = conved.reshape(full_len, seq_count, channels // HEAD_DIM, HEAD_DIM)
    head_mean = jnp.mean(grouped, axis=-1, keepdims=True)
    head_var = jnp.mean(jnp.square(grouped - head_mean), axis=-1, keepdims=True)
    scaled = (
        (grouped - head_mean) * lax.rsqrt(head_var + group_eps) * head_gain.reshape(-1, HEAD_DIM)
    )
    activated = jax.nn.silu(scaled).astype(jnp.bfloat16).reshape(-1, channels)
    out_columns = gather_directly(out_weight, "fs", 1)
    sliced = lax.slice_in_dim(activated, 0, own_rows * lax.axis_size("tp"), axis=0)
    mixed_rows = sent_and_summed(
        jnp.dot(sliced, out_columns, preferred_element_type=jnp.float32).astype(jnp.bfloat16),
        "tp",
        0,
    )
    residual = tokens.reshape(own_rows, model_width).astype(jnp.float32)
    middle = (residual + mixed_rows).astype(jnp.bfloat16)
    middle_whole = gather_directly(middle.reshape(local_len, seq_count, model_width), "tp", 0)
    normed_ffn = rms_scale(
        middle_whole.reshape(-1, model_width).astype(jnp.float32), ffn_gain
    ).astype(jnp.bfloat16)
    pieces = sent_together((ffn_gate_weight, ffn_up_weight), "fs", 0, 1)
    sliced = normed_ffn
    gate_part = jnp.dot(sliced, pieces[0], preferred_element_type=jnp.float32)
    up_part = jnp.dot(sliced, pieces[1], preferred_element_type=jnp.float32)
    hidden = (jax.nn.silu(gate_part) * up_part).astype(jnp.bfloat16)
    down_columns = lax.all_gather(down_weight, "fs", axis=1, tiled=True)
    sliced = hidden
    fed_rows = sent_and_summed(
        jnp.dot(sliced, down_columns, preferred_element_type=jnp.float32).astype(jnp.bfloat16),
        "tp",
        0,
    )
    layer_rows = (middle.astype(jnp.float32) + fed_rows).astype(jnp.bfloat16)
    return layer_rows.reshape(local_len, seq_count, model_width)


def solution(mesh):
    placed = (
        P("tp", ("rep", "fs"), None),
        P(),
        P("fs", "tp"),
        P("fs", "tp"),
        P(None, "tp"),
        P("tp"),
        P("tp", "fs"),
        P(),
        P("fs", "tp"),
        P("fs", "tp"),
        P("tp", "fs"),
    )
    return jax.shard_map(
        body, mesh=mesh, in_specs=placed, out_specs=P("tp", ("rep", "fs"), None), check_vma=False
    )
```

profile of v0, /device:TPU:1, one launch (start us, length us, event | category | flops | bytes accessed | tf_op | source)
XLA Modules:
  0.0 537.6 jit_solution(16612511845772567293)
XLA Ops:
  6.5 1.6 pad_maximum_fusion.1
  8.1 0.0 all-gather.4.cloned.1.call-update
  8.2 0.0 all-gather.6.cloned.1.call-start
  8.2 1.8 pad_maximum_fusion
  10.0 0.0 all-gather.6.cloned.1.call-update
  10.0 0.0 all-gather.8.cloned.1.call-start
  10.1 0.7 all-gather.8.cloned.1.call-update
  10.8 0.1 broadcast_in_dim.11
  10.9 5.6 %all_to_all.25 = bf16[2,128,1,2048]{3,1,2,0:T(8,128)(2,1)S(1)} all-to-all(bf16[2,128,1,2048]{3,1,2,0:T(8,128)(2,1)S(1)} %broadcast_in_dim.11), channel_id=1, replica_groups=mesh['rep'=2,'fs'=32,'tp'=2] {'tp'}, dimensions={0} | all-to-all | bytes 2097152 | tf_op jit(solution)/shard_map/all_to_all | solution.py:13
  16.5 1.6 broadcast_in_dim.13
  18.1 8.6 %all-to-all-start.1 = ((bf16[32,512,64]{1,2,0:T(8,128)(2,1)}), bf16[32,512,64]{1,2,0:T(8,128)(2,1)S(1)}, u32[]{:S(2)}, u32[]{:S(2)}) async-start(bf16[32,512,64]{1,2,0:T(8,128)(2,1)} %broadcast_in_dim.13), calls=%async_computation.1 | async-start | bytes 4194304 | tf_op jit(solution)/shard_map/all_to_all | solution.py:13
  26.7 0.3 multiply_reduce_fusion.1
  27.0 1.3 fusion.17
  28.4 130.0 %all-gather.4.cloned.1.call-done = bf16[2048,1024]{1,0:T(8,128)(2,1)} async-done(((bf16[64,1024]{1,0:T(8,128)(2,1)}), bf16[2048,1024]{1,0:T(8,128)(2,1)}) %all-gather.4.cloned.1.call-update) | async-done | bytes 4194320 | tf_op jit(solution)/shard_map/all_gather | solution.py:31
  158.3 2.8 fusion.35
  161.2 0.3 copy-done.9
  161.5 0.7 fusion.38
  162.2 0.0 copy-start.10
  162.2 0.1 pad
  162.3 0.1 reshape.186
  162.4 0.1 copy.21
  162.5 0.1 slice.20
  162.5 0.4 copy-done.10
  162.9 1.3 convolution_select_fusion
  164.2 0.3 copy.23
  164.6 0.9 reshape.190
  165.5 1.1 slice.21
  166.5 0.0 copy-start.8
  166.5 0.2 reshape.179
  166.7 1.0 reshape.180
  167.7 0.3 reduce_sum.59
  168.1 1.7 multiply_reduce_fusion.2
  169.8 0.8 fusion.51
  170.6 0.7 convolution_convert_fusion
  171.3 23.2 %all_to_all.26 = bf16[2,128,2048]{2,1,0:T(8,128)(2,1)S(1)} all-to-all(bf16[2,128,2048]{2,1,0:T(8,128)(2,1)S(1)} %bitcast.53), channel_id=1, replica_groups=mesh['rep'=2,'fs'=32,'tp'=2] {'tp'}, dimensions={0} | all-to-all | bytes 2097152 | tf_op jit(solution)/shard_map/all_to_all | solution.py:45
  194.5 0.2 convert_reduce_fusion.1
  194.7 0.1 add_convert_fusion
  194.8 0.1 broadcast_in_dim.14
  195.0 4.6 all_to_all.27
  199.6 0.3 multiply_reduce_fusion
  199.9 0.3 fusion.15
  200.2 134.7 %all-gather.6.cloned.1.call-done = bf16[2048,3072]{1,0:T(8,128)(2,1)} async-done(((bf16[64,3072]{1,0:T(8,128)(2,1)}), bf16[2048,3072]{1,0:T(8,128)(2,1)}) %all-gather.6.cloned.1.call-update) | async-done | bytes 12582928 | tf_op jit(solution)/shard_map/all_gather | solution.py:31
  334.9 5.7 %fusion.2 = f32[256,1536]{1,0:T(8,128)} fusion(bf16[256,2048]{1,0:T(8,128)(2,1)S(1)} %fusion.15, bf16[2048,3072]{1,0:T(8,128)(2,1)} %all-gather.6.cloned.1.call-done), kind=kOutput, calls=%fused_computation.2 | convolution fusion | flops 1610612736 | bytes 8912896 | tf_op jit(solution)/shard_map/dot_general | solution.py:115
  340.7 155.1 %all-gather.8.cloned.1.call-done = bf16[1536,2048]{0,1:T(8,128)(2,1)} async-done(((bf16[1536,64]{0,1:T(8,128)(2,1)}), bf16[1536,2048]{0,1:T(8,128)(2,1)}) %all-gather.8.cloned.1.call-update) | async-done | bytes 6291472 | tf_op jit(solution)/shard_map/all_gather | solution.py:118
  495.7 8.8 %convolution_convert_fusion.1 = bf16[256,2048]{1,0:T(8,128)(2,1)S(1)} fusion(bf16[1536,2048]{0,1:T(8,128)(2,1)} %all-gather.8.cloned.1.call-done, bf16[256,2048]{1,0:T(8,128)(2,1)} %copy-done.3, bf16[2048,3072]{1,0:T(8,128)(2,1)} %all-gather.6.cloned.1.call-done, f32[256,1536]{1,0:T(8,128)} %fusion.2), kind=kOutput, calls=%fused_computation.7 | convolution fusion | flops 3224109056 | bytes 16252928 | tf_op jit(solution)/shard_map/dot_general | solution.py:121
  504.5 25.3 %all_to_all.28 = bf16[2,128,2048]{2,1,0:T(8,128)(2,1)S(1)} all-to-all(bf16[2,128,2048]{2,1,0:T(8,128)(2,1)S(1)} %bitcast.54), channel_id=1, replica_groups=mesh['rep'=2,'fs'=32,'tp'=2] {'tp'}, dimensions={0} | all-to-all | bytes 2097152 | tf_op jit(solution)/shard_map/all_to_all | solution.py:45
  529.9 0.2 convert_reduce_fusion
  530.1 1.0 fusion.42
  (24 shorter events, 0.1 us)
Async XLA Ops:
  6.5 156.0 %copy-start = (f32[31,512]{1,0:T(8,128)S(1)}, f32[31,512]{1,0:T(8,128)}, u32[]{:S(2)}) copy-start(f32[31,512]{1,0:T(8,128)} %param.15) | copy-start | bytes 190468
  6.5 4.2 copy-start.1
  6.5 151.8 %all-gather.4.cloned.1.call-start = ((), (), s32[]{:S(2)}) async-start(), calls=%async_computation.5 | async-start | bytes 4325376 | tf_op jit(solution)/shard_map/all_gather | solution.py:31
  8.2 326.8 %all-gather.6.cloned.1.call-start = ((), (), s32[]{:S(2)}) async-start(), calls=%async_computation.6 | async-start | bytes 12976128 | tf_op jit(solution)/shard_map/all_gather | solution.py:31
  10.0 6.5 %copy-start.5 = (bf16[512,64]{0,1:T(8,128)(2,1)S(1)}, bf16[512,64]{0,1:T(8,128)(2,1)}, u32[]{:S(2)}) copy-start(bf16[512,64]{0,1:T(8,128)(2,1)} %param.17) | copy-start | bytes 196612
  10.0 485.7 %all-gather.8.cloned.1.call-start = ((), (), s32[]{:S(2)}) async-start(), calls=%async_computation.7 | async-start | bytes 6488064 | tf_op jit(solution)/shard_map/all_gather | solution.py:118
  18.1 8.9 %copy-start.6 = (f32[2048]{0:T(1024)S(1)}, f32[2048]{0:T(1024)}, u32[]{:S(2)}) copy-start(f32[2048]{0:T(1024)} %param.12) | copy-start | bytes 24580
  18.1 152.5 %all-to-all-start.1 = ((bf16[32,512,64]{1,2,0:T(8,128)(2,1)}), bf16[32,512,64]{1,2,0:T(8,128)(2,1)S(1)}, u32[]{:S(2)}, u32[]{:S(2)}) async-start(bf16[32,512,64]{1,2,0:T(8,128)(2,1)} %broadcast_in_dim.13), calls=%async_computation.1 | async-start | bytes 4194304 | tf_op jit(solution)/shard_map/all_to_all | solution.py:13
  28.4 132.8 %copy-start.4 = (bf16[256,2048]{1,0:T(8,128)(2,1)S(1)}, bf16[256,2048]{1,0:T(8,128)(2,1)}, u32[]{:S(2)}) copy-start(bf16[256,2048]{1,0:T(8,128)(2,1)} %fusion.17) | copy-start | bytes 3145732
  158.3 3.1 copy-start.9
  162.2 0.7 copy-start.10
  166.5 3.3 copy-start.8
  171.3 23.4 %copy-start.2 = (bf16[128,1,2048]{2,0,1:T(8,128)(2,1)S(1)}, bf16[128,1,2048]{2,0,1:T(8,128)(2,1)}, u32[]{:S(2)}) copy-start(bf16[128,1,2048]{2,0,1:T(8,128)(2,1)} %param.11) | copy-start | bytes 1572868
  194.8 5.1 copy-start.7
  200.2 140.4 %copy-start.3 = (bf16[256,2048]{1,0:T(8,128)(2,1)}, bf16[256,2048]{1,0:T(8,128)(2,1)S(1)}, u32[]{:S(2)}) copy-start(bf16[256,2048]{1,0:T(8,128)(2,1)S(1)} %fusion.15) | copy-start | bytes 3145732
Sparse Core Ops, SparseCore 0:
  9.0 149.3 all-gather.3
  160.0 174.9 all-gather.5
  336.6 159.1 all-gather.7
where the time goes:
time: 538 us
  waiting for transfers between devices  420 us (78%)
  blocking collectives  58.7 us (11%)
  matrix products  20.1 us (4%)
  between operations  13.4 us (2%)
  other arithmetic  9.93 us (2%)
  starting transfers between devices  8.72 us (2%)
  local copies, waits for them, and re-layouts  6.23 us (1%)
    all_gather x2, waiting for transfers between devices, sent_together(): lax.all_gather(both, axis, axis=dim, tiled=True)  265 us
    all_gather x1, waiting for transfers between devices, body(): down_columns = lax.all_gather(down_weight, 'fs', axis=1, tiled=True)  155 us
    all_to_all x2, blocking collectives, sent_and_summed(): lax.all_to_all(parts, axis, split_axis=0, concat_axis=0, tiled=True)  48.5 us
  transfers between devices with their start and end apart: 4, of which 3 were waited for; matrix products, arithmetic and copies ran while one was open for 4% of the time, Pallas kernels for 0%

commit v1 on v0

--- a/solution.py
+++ b/solution.py
@@ -115,7 +115,9 @@
     gate_part = jnp.dot(sliced, pieces[0], preferred_element_type=jnp.float32)
     up_part = jnp.dot(sliced, pieces[1], preferred_element_type=jnp.float32)
     hidden = (jax.nn.silu(gate_part) * up_part).astype(jnp.bfloat16)
-    down_columns = lax.all_gather(down_weight, "fs", axis=1, tiled=True)
+    down_columns = jnp.concatenate(
+        lax.all_to_all(jnp.stack([down_weight] * lax.axis_size("fs")), "fs", 0, 0), axis=1
+    )
     sliced = hidden
     fed_rows = sent_and_summed(
         jnp.dot(sliced, down_columns, preferred_element_type=jnp.float32).astype(jnp.bfloat16),

time: 538 us -> 457 us (0.85)
  waiting for transfers between devices: 420 us -> 333 us
  blocking collectives: 58.7 us -> 50.9 us
  starting transfers between devices: 8.72 us -> 16.1 us
    all_gather x1 -> x0, waiting for transfers between devices: 155 us -> none  [body(): down_columns = lax.all_gather(down_weight, 'fs', axis=1, tiled=True)]
    all_gather x2, waiting for transfers between devices: 265 us -> 333 us  [sent_together(): lax.all_gather(both, axis, axis=dim, tiled=True)]
    all_to_all x2, blocking collectives: 48.5 us -> 40.8 us  [sent_and_summed(): lax.all_to_all(parts, axis, split_axis=0, concat_axis=0, tiled=True)]
    all_to_all x0 -> x1, starting transfers between devices: none -> 7.41 us  [body(): lax.all_to_all(jnp.stack([down_weight] * lax.axis_size('fs')), 'fs', 0, 0)]
  transfers between devices with their start and end apart: 4 -> 4, of which waited for: 3 -> 2; matrix products, arithmetic and copies ran while one was open for 4% -> 7% of each run, Pallas kernels for 0% -> 0%
where the time goes in v1:
time: 457 us; the launch traced here: 456 us
  waiting for transfers between devices  333 us (73%)
  blocking collectives  50.9 us (11%)
  matrix products  20.6 us (5%)
  starting transfers between devices  16.1 us (4%)
  between operations  13.7 us (3%)
  other arithmetic  10.9 us (2%)
  local copies, waits for them, and re-layouts  10.6 us (2%)
    all_gather x2, waiting for transfers between devices, sent_together(): lax.all_gather(both, axis, axis=dim, tiled=True)  333 us
    all_to_all x2, blocking collectives, sent_and_summed(): lax.all_to_all(parts, axis, split_axis=0, concat_axis=0, tiled=True)  40.8 us
    all_to_all x2, blocking collectives, from_everyone(): lax.all_to_all(jnp.broadcast_to(value[None], (count, *value.shape)), axis...  10.2 us
  transfers between devices with their start and end apart: 4, of which 2 were waited for; matrix products, arithmetic and copies ran while one was open for 7% of the time, Pallas kernels for 0%

profile of v1, /device:TPU:1, one launch (start us, length us, event | category | flops | bytes accessed | tf_op | source)
XLA Modules:
  0.0 456.1 jit_solution(1332634045347429729)
XLA Ops:
  6.5 1.6 pad_maximum_fusion.1
  8.1 0.0 all-gather.3.cloned.1.call-update
  8.1 0.0 all-gather.5.cloned.1.call-start
  8.2 1.9 pad_maximum_fusion
  10.0 0.0 all-gather.5.cloned.1.call-update
  10.1 1.2 broadcast_in_dim.11
  11.3 5.6 %all_to_all.30 = bf16[2,128,1,2048]{3,1,2,0:T(8,128)(2,1)S(1)} all-to-all(bf16[2,128,1,2048]{3,1,2,0:T(8,128)(2,1)S(1)} %broadcast_in_dim.11), channel_id=1, replica_groups=mesh['rep'=2,'fs'=32,'tp'=2] {'tp'}, dimensions={0} | all-to-all | bytes 2097152 | tf_op jit(solution)/shard_map/all_to_all | solution.py:13
  16.9 1.6 broadcast_in_dim.13
  18.4 8.6 %all-to-all-start.1 = ((bf16[32,512,64]{1,2,0:T(8,128)(2,1)}), bf16[32,512,64]{1,2,0:T(8,128)(2,1)S(1)}, u32[]{:S(2)}, u32[]{:S(2)}) async-start(bf16[32,512,64]{1,2,0:T(8,128)(2,1)} %broadcast_in_dim.13), calls=%async_computation.1 | async-start | bytes 4194304 | tf_op jit(solution)/shard_map/all_to_all | solution.py:13
  27.1 0.3 multiply_reduce_fusion.1
  27.4 1.3 fusion.17
  28.7 130.0 %all-gather.3.cloned.1.call-done = bf16[2048,1024]{1,0:T(8,128)(2,1)} async-done(((bf16[64,1024]{1,0:T(8,128)(2,1)}), bf16[2048,1024]{1,0:T(8,128)(2,1)}) %all-gather.3.cloned.1.call-update) | async-done | bytes 4194320 | tf_op jit(solution)/shard_map/all_gather | solution.py:31
  158.7 2.8 fusion.35
  161.6 0.3 copy-done.8
  161.9 0.7 fusion.38
  162.6 0.0 copy-start.9
  162.6 0.1 pad
  162.7 0.1 reshape.196
  162.8 0.1 copy.22
  162.9 0.1 slice.20
  162.9 0.4 copy-done.9
  163.3 1.3 convolution_select_fusion
  164.6 0.3 copy.24
  164.9 0.9 reshape.200
  165.8 1.1 slice.21
  166.9 0.0 copy-start.7
  166.9 0.2 reshape.187
  167.1 1.0 reshape.188
  168.1 0.3 reduce_sum.59
  168.5 1.7 multiply_reduce_fusion.2
  170.2 0.8 fusion.51
  171.0 0.7 convolution_convert_fusion
  171.7 23.4 %all_to_all.31 = bf16[2,128,2048]{2,1,0:T(8,128)(2,1)S(1)} all-to-all(bf16[2,128,2048]{2,1,0:T(8,128)(2,1)S(1)} %bitcast.56), channel_id=1, replica_groups=mesh['rep'=2,'fs'=32,'tp'=2] {'tp'}, dimensions={0} | all-to-all | bytes 2097152 | tf_op jit(solution)/shard_map/all_to_all | solution.py:45
  195.1 0.2 convert_reduce_fusion.1
  195.3 0.1 add_convert_fusion
  195.4 0.0 copy-start.3
  195.4 0.1 broadcast_in_dim.14
  195.6 4.6 %all_to_all.32 = bf16[2,128,1,2048]{3,1,2,0:T(8,128)(2,1)S(1)} all-to-all(bf16[2,128,1,2048]{3,1,2,0:T(8,128)(2,1)S(1)} %broadcast_in_dim.14), channel_id=1, replica_groups=mesh['rep'=2,'fs'=32,'tp'=2] {'tp'}, dimensions={0} | all-to-all | bytes 2097152 | tf_op jit(solution)/shard_map/all_to_all | solution.py:13
  200.1 3.3 stack.2
  203.5 7.4 %all-to-all-start.4 = ((bf16[32,1536,64]{1,2,0:T(8,128)(2,1)}), bf16[32,1536,64]{1,2,0:T(8,128)(2,1)}, u32[]{:S(2)}, u32[]{:S(2)}) async-start(bf16[32,1536,64]{1,2,0:T(8,128)(2,1)} %stack.2), calls=%async_computation.4 | async-start | bytes 12582912 | tf_op jit(solution)/shard_map/all_to_all | solution.py:119
  210.9 0.3 multiply_reduce_fusion
  211.2 1.3 fusion.15
  212.5 203.3 %all-gather.5.cloned.1.call-done = bf16[2048,3072]{1,0:T(8,128)(2,1)} async-done(((bf16[64,3072]{1,0:T(8,128)(2,1)}), bf16[2048,3072]{1,0:T(8,128)(2,1)}) %all-gather.5.cloned.1.call-update) | async-done | bytes 12582928 | tf_op jit(solution)/shard_map/all_gather | solution.py:31
  415.7 6.1 %fusion.2 = f32[256,1536]{1,0:T(8,128)} fusion(bf16[256,2048]{1,0:T(8,128)(2,1)} %fusion.15, bf16[2048,3072]{1,0:T(8,128)(2,1)} %all-gather.5.cloned.1.call-done), kind=kOutput, calls=%fused_computation.2 | convolution fusion | flops 1610612736 | bytes 8912896 | tf_op jit(solution)/shard_map/dot_general | solution.py:115
  421.9 8.8 %convolution_convert_fusion.1 = bf16[256,2048]{1,0:T(8,128)(2,1)S(1)} fusion(bf16[1536,2048]{0,1:T(8,128)(2,1)} %bitcast.14, bf16[256,2048]{1,0:T(8,128)(2,1)} %fusion.15, bf16[2048,3072]{1,0:T(8,128)(2,1)} %all-gather.5.cloned.1.call-done, f32[256,1536]{1,0:T(8,128)} %fusion.2), kind=kOutput, calls=%fused_computation.7 | convolution fusion | flops 3224109056 | bytes 16252928 | tf_op jit(solution)/shard_map/dot_general | solution.py:123
  430.7 17.4 %all_to_all.33 = bf16[2,128,2048]{2,1,0:T(8,128)(2,1)S(1)} all-to-all(bf16[2,128,2048]{2,1,0:T(8,128)(2,1)S(1)} %bitcast.57), channel_id=1, replica_groups=mesh['rep'=2,'fs'=32,'tp'=2] {'tp'}, dimensions={0} | all-to-all | bytes 2097152 | tf_op jit(solution)/shard_map/all_to_all | solution.py:45
  448.1 0.2 convert_reduce_fusion
  448.3 1.0 fusion.42
  (22 shorter events, 0.1 us)
Async XLA Ops:
  6.5 156.4 %copy-start = (f32[31,512]{1,0:T(8,128)S(1)}, f32[31,512]{1,0:T(8,128)}, u32[]{:S(2)}) copy-start(f32[31,512]{1,0:T(8,128)} %param.15) | copy-start | bytes 190468
  6.5 152.2 %all-gather.3.cloned.1.call-start = ((), (), s32[]{:S(2)}) async-start(), calls=%async_computation.6 | async-start | bytes 4325376 | tf_op jit(solution)/shard_map/all_gather | solution.py:31
  8.1 407.6 %all-gather.5.cloned.1.call-start = ((), (), s32[]{:S(2)}) async-start(), calls=%async_computation.7 | async-start | bytes 12976128 | tf_op jit(solution)/shard_map/all_gather | solution.py:31
  10.0 6.8 %copy-start.4 = (bf16[512,64]{0,1:T(8,128)(2,1)S(1)}, bf16[512,64]{0,1:T(8,128)(2,1)}, u32[]{:S(2)}) copy-start(bf16[512,64]{0,1:T(8,128)(2,1)} %param.17) | copy-start | bytes 196612
  18.4 8.9 %copy-start.5 = (f32[2048]{0:T(1024)S(1)}, f32[2048]{0:T(1024)}, u32[]{:S(2)}) copy-start(f32[2048]{0:T(1024)} %param.12) | copy-start | bytes 24580
  18.4 152.5 %all-to-all-start.1 = ((bf16[32,512,64]{1,2,0:T(8,128)(2,1)}), bf16[32,512,64]{1,2,0:T(8,128)(2,1)S(1)}, u32[]{:S(2)}, u32[]{:S(2)}) async-start(bf16[32,512,64]{1,2,0:T(8,128)(2,1)} %broadcast_in_dim.13), calls=%async_computation.1 | async-start | bytes 4194304 | tf_op jit(solution)/shard_map/all_to_all | solution.py:13
  28.7 132.9 %copy-start.2 = (bf16[256,2048]{1,0:T(8,128)(2,1)S(1)}, bf16[256,2048]{1,0:T(8,128)(2,1)}, u32[]{:S(2)}) copy-start(bf16[256,2048]{1,0:T(8,128)(2,1)} %fusion.17) | copy-start | bytes 3145732
  158.7 3.1 copy-start.8
  162.6 0.7 copy-start.9
  166.9 3.3 copy-start.7
  171.7 23.6 %copy-start.1 = (bf16[128,1,2048]{2,0,1:T(8,128)(2,1)S(1)}, bf16[128,1,2048]{2,0,1:T(8,128)(2,1)}, u32[]{:S(2)}) copy-start(bf16[128,1,2048]{2,0,1:T(8,128)(2,1)} %param.11) | copy-start | bytes 1572868
  195.4 4.7 %copy-start.3 = (bf16[1536,64]{0,1:T(8,128)(2,1)S(1)}, bf16[1536,64]{0,1:T(8,128)(2,1)}, u32[]{:S(2)}) copy-start(bf16[1536,64]{0,1:T(8,128)(2,1)} %param.21) | copy-start | bytes 589828
  203.5 7.7 %copy-start.6 = (f32[2048]{0:T(1024)S(1)}, f32[2048]{0:T(1024)}, u32[]{:S(2)}) copy-start(f32[2048]{0:T(1024)} %param.18) | copy-start | bytes 24580
  203.5 218.4 %all-to-all-start.4 = ((bf16[32,1536,64]{1,2,0:T(8,128)(2,1)}), bf16[32,1536,64]{1,2,0:T(8,128)(2,1)}, u32[]{:S(2)}, u32[]{:S(2)}) async-start(bf16[32,1536,64]{1,2,0:T(8,128)(2,1)} %stack.2), calls=%async_computation.4 | async-start | bytes 12582912 | tf_op jit(solution)/shard_map/all_to_all | solution.py:119
Sparse Core Ops, SparseCore 0:
  9.0 149.7 all-gather.2
  160.4 255.3 all-gather.4
